TPU v7x, 32 devices: a whole 2x2x4 slice. The times are simulated.
32 devices in a mesh: fs: 8 (over z, y), tp: 4 (over x, core).
Axes of the slice: x: 2, y: 2, z: 4, core: 2. Of those that a mesh axis runs over, the one named last changes fastest.
Arguments:
- prompt_tokens: bfloat16 [768, 4096], P('tp'), may hold values from -6 to 6
- norm_gain: float32 [4096], P('fs'), may hold values from 0.1 to 1.9
- gate_trained: float32 [4096, 11264], P('fs', 'tp'), may hold values from -0.09375 to 0.09375
- up_trained: float32 [4096, 11264], P('fs', 'tp'), may hold values from -0.09375 to 0.09375
- down_trained: float32 [11264, 4096], P('fs', 'tp'), may hold values from -0.078125 to 0.078125
Outputs:
- gate_serving: bfloat16 [4096, 11264], P(None, 'fs')
- up_serving: bfloat16 [4096, 11264], P(None, 'fs')
- down_serving: bfloat16 [11264, 4096], P('fs')
- mixed: bfloat16 [768, 4096], P('tp', 'fs')
All inputs are finite; a program needn't handle non-finite values.
Results may differ from a plain program's by a relative error of at most 0.0082.
Values may be sent and summed in bfloat16 or wider, within the bound.
A program may use at most 128 MiB of HBM per device.

v0:
```python
import jax
import jax.numpy as jnp
from jax import lax
from jax.sharding import PartitionSpec as P


def on_device(prompt_tokens, norm_gain, gate_trained, up_trained, down_trained):
    fs_count = lax.axis_size("fs")
    gate_cast = (gate_trained * norm_gain[:, None]).astype(jnp.bfloat16)
    up_cast = (up_trained * norm_gain[:, None]).astype(jnp.bfloat16)
    down_cast = down_trained.astype(jnp.bfloat16)
    down_serving = lax.all_gather(down_cast, "tp", axis=1, tiled=True)
    gate_part, up_part = (
        lax.all_to_all(gate_cast, "tp", split_axis=0, concat_axis=1, tiled=True),
        lax.all_to_all(up_cast, "tp", split_axis=0, concat_axis=1, tiled=True),
    )
    gate_mid, up_mid = (
        lax.all_to_all(gate_part, "fs", split_axis=1, concat_axis=0, tiled=True),
        lax.all_to_all(up_part, "fs", split_axis=1, concat_axis=0, tiled=True),
    )
    share = gate_mid.shape[0] // fs_count
    width = gate_mid.shape[1]
    gate_blocks, up_blocks = (
        lax.all_gather(gate_mid.reshape(fs_count, share, width), "tp", axis=1, tiled=True),
        lax.all_gather(up_mid.reshape(fs_count, share, width), "tp", axis=1, tiled=True),
    )
    gate_serving = gate_blocks.reshape(-1, width)
    up_serving = up_blocks.reshape(-1, width)
    tokens = prompt_tokens.astype(jnp.float32)
    scale = lax.rsqrt(jnp.mean(tokens * tokens, axis=-1, keepdims=True) + 1e-06)
    normed = (tokens * scale).astype(jnp.bfloat16)
    contract = (((0,), (1,)), ((), ()))
    gate_cols = lax.dot_general(gate_serving, normed, contract, preferred_element_type=jnp.float32)
    up_cols = lax.dot_general(up_serving, normed, contract, preferred_element_type=jnp.float32)
    hidden_cols = (jax.nn.silu(gate_cols) * up_cols).astype(jnp.bfloat16)
    summed = lax.psum_scatter(
        lax.dot_general(
            down_serving, hidden_cols, (((0,), (0,)), ((), ())), preferred_element_type=jnp.float32
        ),
        "fs",
        scatter_dimension=0,
        tiled=True,
    )
    mixed = summed.T.astype(jnp.bfloat16)
    return (gate_serving, up_serving, down_serving, mixed)


def solution(mesh):
    return jax.shard_map(
        on_device,
        mesh=mesh,
        in_specs=(P("tp", None), P("fs"), P("fs", "tp"), P("fs", "tp"), P("fs", "tp")),
        out_specs=(P(None, "fs"), P(None, "fs"), P("fs", None), P("tp", "fs")),
        check_vma=False,
    )
```

profile of v0, /device:TPU:0, one launch (start us, length us, event | category | flops | bytes accessed | tf_op | source)
XLA Modules:
  0.0 524.6 jit_solution(6554279546055345411)
XLA Ops:
  7.2 0.0 all-gather.4.cloned.1.call-start
  7.2 5.5 %multiply_convert_fusion = (bf16[512,2816]{1,0:T(8,128)(2,1)S(1)}, bf16[512,2816]{1,0:T(8,128)(2,1)S(1)}) fusion(f32[512,2816]{1,0:T(8,128)} %param.8, f32[512]{0:T(512)} %param.6, f32[512,2816]{1,0:T(8,128)} %param.7), kind=kLoop, calls=%fused_computation | loop fusion | flops 5767168 | bytes 17303552 | tf_op jit(solution)/shard_map/convert_element_type | solution.py:10
  12.7 38.2 %all_to_all.64 = bf16[4,128,2816]{2,1,0:T(8,128)(2,1)} all-to-all(bf16[4,128,2816]{2,1,0:T(8,128)(2,1)S(1)} %bitcast.18), channel_id=1, replica_groups=mesh['fs'=8,'tp'=4] {'tp'}, dimensions={0} | all-to-all | bytes 5767168 | tf_op jit(solution)/shard_map/all_to_all | solution.py:14
  51.0 4.5 copy.9
  55.5 71.4 %all_to_all.65 = bf16[128,8,1408]{0,2,1:T(8,128)(2,1)} all-to-all(bf16[128,8,1408]{0,2,1:T(8,128)(2,1)} %bitcast.26), channel_id=1, replica_groups=mesh['fs'=8,'tp'=4] {'fs'}, dimensions={1} | all-to-all | bytes 5767168 | tf_op jit(solution)/shard_map/all_to_all | solution.py:18
  126.9 0.0 all-gather.4.cloned.1.call-update
  126.9 0.0 all-gather.6.cloned.1.call-start
  127.0 64.5 %all_to_all.66 = bf16[4,128,2816]{2,1,0:T(8,128)(2,1)} all-to-all(bf16[4,128,2816]{2,1,0:T(8,128)(2,1)S(1)} %bitcast.17), channel_id=1, replica_groups=mesh['fs'=8,'tp'=4] {'tp'}, dimensions={0} | all-to-all | bytes 5767168 | tf_op jit(solution)/shard_map/all_to_all | solution.py:15
  191.5 3.3 copy.11
  194.8 67.9 %all_to_all.67 = bf16[128,8,1408]{0,2,1:T(8,128)(2,1)} all-to-all(bf16[128,8,1408]{0,2,1:T(8,128)(2,1)S(1)} %bitcast.28), channel_id=1, replica_groups=mesh['fs'=8,'tp'=4] {'fs'}, dimensions={1} | all-to-all | bytes 5767168 | tf_op jit(solution)/shard_map/all_to_all | solution.py:19
  262.7 0.0 all-gather.6.cloned.1.call-update
  262.8 0.0 all-gather.8.cloned.1.call-start
  262.8 4.7 convert_element_type.26
  267.5 0.0 copy-start
  267.5 0.0 all-gather.8.cloned.1.call-update
  267.5 0.0 reduce-scatter.2.cloned.1.call-start
  267.6 1.6 copy-done
  269.1 0.4 fusion
  269.5 0.0 all-gather.4.cloned.1.call-done
  269.6 16.0 %copy.10 = bf16[8,512,1408]{2,1,0:T(8,128)(2,1)} copy(bf16[8,512,1408]{1,2,0:T(8,128)(2,1)} %all-gather.4.cloned.1.call-done) | data formatting | bytes 23068672 | tf_op jit(solution)/shard_map/all_gather | solution.py:24
  285.6 53.0 %all-gather.6.cloned.1.call-done = bf16[8,512,1408]{1,2,0:T(8,128)(2,1)} async-done(((bf16[8,128,1408]{1,2,0:T(8,128)(2,1)}), bf16[8,512,1408]{1,2,0:T(8,128)(2,1)}) %all-gather.6.cloned.1.call-update) | async-done | bytes 11534352 | tf_op jit(solution)/shard_map/all_gather | solution.py:25
  338.5 16.0 %copy.12 = bf16[8,512,1408]{2,1,0:T(8,128)(2,1)} copy(bf16[8,512,1408]{1,2,0:T(8,128)(2,1)} %all-gather.6.cloned.1.call-done) | data formatting | bytes 23068672 | tf_op jit(solution)/shard_map/all_gather | solution.py:25
  354.5 7.2 %fusion.3 = f32[1408,192]{0,1:T(8,128)S(1)} fusion(bf16[4096,1408]{1,0:T(8,128)(2,1)} %bitcast.19, bf16[192,4096]{1,0:T(8,128)(2,1)S(1)} %copy-done, f32[192]{0:T(256)S(1)} %add_rsqrt_fusion), kind=kOutput, calls=%fused_computation.9 | convolution fusion | flops 2216951808 | bytes 14189312 | tf_op jit(solution)/shard_map/dot_general | solution.py:33
  361.8 55.1 %all-gather.8.cloned.1.call-done = bf16[1408,4096]{1,0:T(8,128)(2,1)} async-done(((bf16[1408,1024]{1,0:T(8,128)(2,1)}), bf16[1408,4096]{1,0:T(8,128)(2,1)}) %all-gather.8.cloned.1.call-update) | async-done | bytes 11534352 | tf_op jit(solution)/shard_map/all_gather | solution.py:12
  416.8 14.4 %convolution_bitcast_fusion = f32[4096,192]{0,1:T(8,128)} fusion(bf16[1408,4096]{1,0:T(8,128)(2,1)} %all-gather.8.cloned.1.call-done, bf16[4096,1408]{1,0:T(8,128)(2,1)} %bitcast.21, f32[1408,192]{0,1:T(8,128)S(1)} %fusion.3, bf16[192,4096]{1,0:T(8,128)(2,1)S(1)} %copy-done, f32[192]{0:T(256)S(1)} %add_rsqrt_fusion), kind=kOutput, calls=%fused_computation.2 | convolution fusion | flops 4433166336 | bytes 28869376 | tf_op jit(solution)/shard_map/dot_general | solution.py:37
  431.3 0.0 reduce-scatter.2.cloned.1.call-update
  431.3 75.0 %reduce-scatter.2.cloned.1.call-done = f32[512,192]{0,1:T(8,128)} async-done(((f32[4096,192]{0,1:T(8,128)}), f32[512,192]{0,1:T(8,128)}) %reduce-scatter.2.cloned.1.call-update) | async-done | bytes 393232 | tf_op jit(solution)/shard_map/reduce_scatter | solution.py:36
  506.3 1.7 convert_bitcast_fusion
  508.0 10.1 %copy.14 = bf16[1408,4096]{1,0:T(8,128)(2,1)} copy(bf16[1408,4096]{1,0:T(8,128)(2,1)} %all-gather.8.cloned.1.call-done) | data formatting | bytes 23068672
  (1 shorter events, 0.0 us)
Async XLA Ops:
  7.2 262.4 %all-gather.4.cloned.1.call-start = ((), (), s32[]{:S(2)}) async-start(), calls=%async_computation.5 | async-start | bytes 14417920 | tf_op jit(solution)/shard_map/all_gather | solution.py:24
  126.9 211.6 %all-gather.6.cloned.1.call-start = ((), (), s32[]{:S(2)}) async-start(), calls=%async_computation.6 | async-start | bytes 14417920 | tf_op jit(solution)/shard_map/all_gather | solution.py:25
  262.8 154.1 %all-gather.8.cloned.1.call-start = ((), (), s32[]{:S(2)}) async-start(), calls=%async_computation.7 | async-start | bytes 14417920 | tf_op jit(solution)/shard_map/all_gather | solution.py:12
  267.5 1.6 copy-start
  267.5 238.8 %reduce-scatter.2.cloned.1.call-start = ((), (), s32[]{:S(2)}) async-start(), calls=%async_computation.8 | async-start | bytes 3538944 | tf_op jit(solution)/shard_map/reduce_scatter | solution.py:36
Sparse Core Ops, SparseCore 0:
  127.1 102.4 all-gather.3
  262.9 75.5 all-gather.5
  340.7 76.1 all-gather.7
  431.4 74.8 reduce-scatter.1
where the time goes:
time: 526 us; the launch traced here: 525 us
  blocking collectives  242 us (46%)
  waiting for transfers between devices  183 us (35%)
  local copies, waits for them, and re-layouts  51.5 us (10%)
  matrix products  21.7 us (4%)
  between operations  13.8 us (3%)
  other arithmetic  12.3 us (2%)
    reduce_scatter x1, waiting for transfers between devices, on_device(): lax.psum_scatter(lax.dot_general(down_serving, hidden_cols, (((0,), (0,))...  75 us
    all_to_all x1, blocking collectives, on_device(): lax.all_to_all(gate_part, 'fs', split_axis=1, concat_axis=0, tiled=True)  71.4 us
    all_to_all x1, blocking collectives, on_device(): lax.all_to_all(up_part, 'fs', split_axis=1, concat_axis=0, tiled=True)  67.9 us
    all_to_all x1, blocking collectives, on_device(): lax.all_to_all(up_cast, 'tp', split_axis=0, concat_axis=1, tiled=True)  64.5 us
    all_gather x1, waiting for transfers between devices, on_device(): down_serving = lax.all_gather(down_cast, 'tp', axis=1, tiled=True)  55.1 us
    all_gather x1, waiting for transfers between devices, on_device(): lax.all_gather(up_mid.reshape(fs_count, share, width), 'tp', axis=1, tile...  53 us
    all_to_all x1, blocking collectives, on_device(): lax.all_to_all(gate_cast, 'tp', split_axis=0, concat_axis=1, tiled=True)  38.2 us
    all_gather x1, local copies, waits for them, and re-layouts, on_device(): lax.all_gather(up_mid.reshape(fs_count, share, width), 'tp', axis=1, tile...  16 us
  transfers between devices with their start and end apart: 4, of which 3 were waited for; matrix products, arithmetic and copies ran while one was open for 9% of the time, Pallas kernels for 0%

commit v1 on v0

--- a/solution.py
+++ b/solution.py
@@ -2,6 +2,13 @@
 import jax.numpy as jnp
 from jax import lax
 from jax.sharding import PartitionSpec as P
+
+
+def stacked_exchange(block, mesh_axis, split, join):
+    devices = lax.axis_size(mesh_axis)
+    pieces = jnp.stack(jnp.split(block, devices, axis=split), axis=0)
+    pieces = lax.all_to_all(pieces, mesh_axis, split_axis=0, concat_axis=0)
+    return jnp.concatenate(pieces, axis=join)
 
 
 def on_device(prompt_tokens, norm_gain, gate_trained, up_trained, down_trained):
@@ -12,7 +19,7 @@
     down_serving = lax.all_gather(down_cast, "tp", axis=1, tiled=True)
     gate_part, up_part = (
         lax.all_to_all(gate_cast, "tp", split_axis=0, concat_axis=1, tiled=True),
-        lax.all_to_all(up_cast, "tp", split_axis=0, concat_axis=1, tiled=True),
+        stacked_exchange(up_cast, "tp", 0, 1),
     )
     gate_mid, up_mid = (
         lax.all_to_all(gate_part, "fs", split_axis=1, concat_axis=0, tiled=True),

time: 526 us -> 527 us (level)
    all_gather x1, waiting for transfers between devices: 0.02 us -> 53 us  [on_device(): lax.all_gather(gate_mid.reshape(fs_count, share, width), 'tp', axis=1, ti...]
    all_gather x1, waiting for transfers between devices: 53 us -> 0.02 us  [on_device(): lax.all_gather(up_mid.reshape(fs_count, share, width), 'tp', axis=1, tile...]
    all_to_all x1, blocking collectives: 64.5 us -> 38.2 us  [stacked_exchange(): pieces = lax.all_to_all(pieces, mesh_axis, split_axis=0, concat_axis=0)]
    all_to_all x1, blocking collectives: 38.2 us -> 64.5 us  [on_device(): lax.all_to_all(gate_cast, 'tp', split_axis=0, concat_axis=1, tiled=True)]
where the time goes in v1:
time: 527 us; the launch traced here: 525 us
  blocking collectives  242 us (46%)
  waiting for transfers between devices  183 us (35%)
  local copies, waits for them, and re-layouts  51.7 us (10%)
  matrix products  21.7 us (4%)
  between operations  13.8 us (3%)
  other arithmetic  12.7 us (2%)
    reduce_scatter x1, waiting for transfers between devices, on_device(): lax.psum_scatter(lax.dot_general(down_serving, hidden_cols, (((0,), (0,))...  74.9 us
    all_to_all x1, blocking collectives, on_device(): lax.all_to_all(up_part, 'fs', split_axis=1, concat_axis=0, tiled=True)  71.4 us
    all_to_all x1, blocking collectives, on_device(): lax.all_to_all(gate_part, 'fs', split_axis=1, concat_axis=0, tiled=True)  67.9 us
    all_to_all x1, blocking collectives, on_device(): lax.all_to_all(gate_cast, 'tp', split_axis=0, concat_axis=1, tiled=True)  64.5 us
    all_gather x1, waiting for transfers between devices, on_device(): down_serving = lax.all_gather(down_cast, 'tp', axis=1, tiled=True)  55.1 us
    all_gather x1, waiting for transfers between devices, on_device(): lax.all_gather(gate_mid.reshape(fs_count, share, width), 'tp', axis=1, ti...  53 us
    all_to_all x1, blocking collectives, stacked_exchange(): pieces = lax.all_to_all(pieces, mesh_axis, split_axis=0, concat_axis=0)  38.2 us
    all_gather x1, local copies, waits for them, and re-layouts, on_device(): lax.all_gather(gate_mid.reshape(fs_count, share, width), 'tp', axis=1, ti...  16 us
  transfers between devices with their start and end apart: 4, of which 3 were waited for; matrix products, arithmetic and copies ran while one was open for 9% of the time, Pallas kernels for 0%

profile of v1, /device:TPU:0, one launch (start us, length us, event | category | flops | bytes accessed | tf_op | source)
XLA Modules:
  0.0 525.1 jit_solution(10907129693258896860)
XLA Ops:
  7.2 0.0 all-gather.6.cloned.1.call-start
  7.2 5.5 %multiply_convert_fusion = (bf16[512,2816]{1,0:T(8,128)(2,1)S(1)}, bf16[512,2816]{1,0:T(8,128)(2,1)S(1)}) fusion(f32[512,2816]{1,0:T(8,128)} %param.8, f32[512]{0:T(512)} %param.6, f32[512,2816]{1,0:T(8,128)} %param.7), kind=kLoop, calls=%fused_computation | loop fusion | flops 5767168 | bytes 17303552 | tf_op jit(solution)/shard_map/convert_element_type | solution.py:17
  12.7 0.2 slice_bitcast_fusion.3
  12.9 0.4 pad_maximum_fusion
  13.3 38.2 %all_to_all.53 = bf16[4,128,2816]{2,1,0:T(8,128)(2,1)} all-to-all(bf16[4,128,2816]{2,1,0:T(8,128)(2,1)S(1)} %pad_maximum_fusion), channel_id=1, replica_groups=mesh['fs'=8,'tp'=4] {'tp'}, dimensions={0} | all-to-all | bytes 5767168 | tf_op jit(solution)/shard_map/all_to_all | solution.py:10
  51.6 4.5 copy.13
  56.1 71.4 %all_to_all.54 = bf16[128,8,1408]{0,2,1:T(8,128)(2,1)} all-to-all(bf16[128,8,1408]{0,2,1:T(8,128)(2,1)} %bitcast.32), channel_id=1, replica_groups=mesh['fs'=8,'tp'=4] {'fs'}, dimensions={1} | all-to-all | bytes 5767168 | tf_op jit(solution)/shard_map/all_to_all | solution.py:26
  127.6 0.0 all-gather.6.cloned.1.call-update
  127.6 0.0 all-gather.4.cloned.1.call-start
  127.6 64.5 %all_to_all.55 = bf16[4,128,2816]{2,1,0:T(8,128)(2,1)} all-to-all(bf16[4,128,2816]{2,1,0:T(8,128)(2,1)S(1)} %bitcast.24), channel_id=1, replica_groups=mesh['fs'=8,'tp'=4] {'tp'}, dimensions={0} | all-to-all | bytes 5767168 | tf_op jit(solution)/shard_map/all_to_all | solution.py:21
  192.1 3.3 copy.11
  195.4 67.9 %all_to_all.56 = bf16[128,8,1408]{0,2,1:T(8,128)(2,1)} all-to-all(bf16[128,8,1408]{0,2,1:T(8,128)(2,1)S(1)} %bitcast.34), channel_id=1, replica_groups=mesh['fs'=8,'tp'=4] {'fs'}, dimensions={1} | all-to-all | bytes 5767168 | tf_op jit(solution)/shard_map/all_to_all | solution.py:25
  263.4 0.0 all-gather.4.cloned.1.call-update
  263.4 0.0 all-gather.8.cloned.1.call-start
  263.4 4.7 convert_element_type.26
  268.1 0.0 copy-start
  268.1 0.0 all-gather.8.cloned.1.call-update
  268.1 0.0 reduce-scatter.2.cloned.1.call-start
  268.2 1.6 copy-done
  269.8 0.4 fusion
  270.2 0.0 all-gather.6.cloned.1.call-done
  270.2 16.0 %copy.14 = bf16[8,512,1408]{2,1,0:T(8,128)(2,1)} copy(bf16[8,512,1408]{1,2,0:T(8,128)(2,1)} %all-gather.6.cloned.1.call-done) | data formatting | bytes 23068672 | tf_op jit(solution)/shard_map/all_gather | solution.py:32
  286.2 53.0 %all-gather.4.cloned.1.call-done = bf16[8,512,1408]{1,2,0:T(8,128)(2,1)} async-done(((bf16[8,128,1408]{1,2,0:T(8,128)(2,1)}), bf16[8,512,1408]{1,2,0:T(8,128)(2,1)}) %all-gather.4.cloned.1.call-update) | async-done | bytes 11534352 | tf_op jit(solution)/shard_map/all_gather | solution.py:31
  339.2 16.0 %copy.12 = bf16[8,512,1408]{2,1,0:T(8,128)(2,1)} copy(bf16[8,512,1408]{1,2,0:T(8,128)(2,1)} %all-gather.4.cloned.1.call-done) | data formatting | bytes 23068672 | tf_op jit(solution)/shard_map/all_gather | solution.py:31
  355.2 7.2 %fusion.3 = f32[1408,192]{0,1:T(8,128)S(1)} fusion(bf16[4096,1408]{1,0:T(8,128)(2,1)} %bitcast.27, bf16[192,4096]{1,0:T(8,128)(2,1)S(1)} %copy-done, f32[192]{0:T(256)S(1)} %add_rsqrt_fusion), kind=kOutput, calls=%fused_computation.14 | convolution fusion | flops 2216951808 | bytes 14189312 | tf_op jit(solution)/shard_map/dot_general | solution.py:40
  362.4 55.1 %all-gather.8.cloned.1.call-done = bf16[1408,4096]{1,0:T(8,128)(2,1)} async-done(((bf16[1408,1024]{1,0:T(8,128)(2,1)}), bf16[1408,4096]{1,0:T(8,128)(2,1)}) %all-gather.8.cloned.1.call-update) | async-done | bytes 11534352 | tf_op jit(solution)/shard_map/all_gather | solution.py:19
  417.5 14.4 %convolution_bitcast_fusion = f32[4096,192]{0,1:T(8,128)} fusion(bf16[1408,4096]{1,0:T(8,128)(2,1)} %all-gather.8.cloned.1.call-done, bf16[4096,1408]{1,0:T(8,128)(2,1)} %bitcast.25, f32[1408,192]{0,1:T(8,128)S(1)} %fusion.3, bf16[192,4096]{1,0:T(8,128)(2,1)S(1)} %copy-done, f32[192]{0:T(256)S(1)} %add_rsqrt_fusion), kind=kOutput, calls=%fused_computation.2 | convolution fusion | flops 4433166336 | bytes 28869376 | tf_op jit(solution)/shard_map/dot_general | solution.py:44
  431.9 0.0 reduce-scatter.2.cloned.1.call-update
  431.9 74.9 %reduce-scatter.2.cloned.1.call-done = f32[512,192]{0,1:T(8,128)} async-done(((f32[4096,192]{0,1:T(8,128)}), f32[512,192]{0,1:T(8,128)}) %reduce-scatter.2.cloned.1.call-update) | async-done | bytes 393232 | tf_op jit(solution)/shard_map/reduce_scatter | solution.py:43
  506.8 1.7 convert_bitcast_fusion
  508.5 10.1 %copy.16 = bf16[1408,4096]{1,0:T(8,128)(2,1)} copy(bf16[1408,4096]{1,0:T(8,128)(2,1)} %all-gather.8.cloned.1.call-done) | data formatting | bytes 23068672
  (1 shorter events, 0.0 us)
Async XLA Ops:
  7.2 263.0 %all-gather.6.cloned.1.call-start = ((), (), s32[]{:S(2)}) async-start(), calls=%async_computation.6 | async-start | bytes 14417920 | tf_op jit(solution)/shard_map/all_gather | solution.py:32
  127.6 211.6 %all-gather.4.cloned.1.call-start = ((), (), s32[]{:S(2)}) async-start(), calls=%async_computation.5 | async-start | bytes 14417920 | tf_op jit(solution)/shard_map/all_gather | solution.py:31
  263.4 154.1 %all-gather.8.cloned.1.call-start = ((), (), s32[]{:S(2)}) async-start(), calls=%async_computation.7 | async-start | bytes 14417920 | tf_op jit(solution)/shard_map/all_gather | solution.py:19
  268.1 1.6 copy-start
  268.1 238.7 %reduce-scatter.2.cloned.1.call-start = ((), (), s32[]{:S(2)}) async-start(), calls=%async_computation.8 | async-start | bytes 3538944 | tf_op jit(solution)/shard_map/reduce_scatter | solution.py:43
Sparse Core Ops, SparseCore 0:
  127.7 102.4 all-gather.5
  263.5 75.5 all-gather.3
  341.3 76.1 all-gather.7
  432.0 74.7 reduce-scatter.1
